TPU v7x, 512 devices: a whole 4x4x16 slice. The times are simulated.
512 devices in a mesh: dp: 4 (over x), kv: 64 (over z, y), tp: 2 (over core).
Axes of the slice: x: 4, y: 4, z: 16, core: 2. Of those that a mesh axis runs over, the one named last changes fastest.
Arguments:
- stream: bfloat16 [512, 2048], P('dp', ('kv', 'tp')), parts along dimension 0, may hold values from -40 to 40
- old_state: float32 [512, 8, 64, 128], P(('dp', 'kv'), 'tp'), parts along dimension 0, may hold values from -6 to 6
- decay_amounts: float32 [512, 512], P(('dp', 'kv'), 'tp'), parts along dimension 0, may hold values from 0.003 to 1
- first_gain: float32 [2048], replicated, may hold values from 0.1 to 1.9
- first_gate: bfloat16 [2048, 5632], P(None, ('kv', 'tp')), may hold values from -0.125 to 0.125
- first_up: bfloat16 [2048, 5632], P(None, ('kv', 'tp')), may hold values from -0.125 to 0.125
- first_down: bfloat16 [5632, 2048], P(('kv', 'tp')), may hold values from -0.078125 to 0.078125
- mixer_gain: float32 [2048], P('kv'), may hold values from 0.1 to 1.9
- query_weight: bfloat16 [2048, 512], P('kv', 'tp'), may hold values from -0.125 to 0.125
- key_weight: bfloat16 [2048, 512], P('kv', 'tp'), may hold values from -0.125 to 0.125
- decay_weight: bfloat16 [2048, 512], P('kv', 'tp'), may hold values from -0.5 to 0.5
- value_weight: bfloat16 [2048, 1024], P('kv', 'tp'), may hold values from -0.125 to 0.125
- output_gate_weight: bfloat16 [2048, 1024], P('kv', 'tp'), may hold values from -0.125 to 0.125
- head_gain: float32 [1024], P('tp'), may hold values from 0.1 to 1.9
- output_weight: bfloat16 [1024, 2048], P('tp', 'kv'), may hold values from -0.1875 to 0.1875
- second_gain: float32 [2048], replicated, may hold values from 0.1 to 1.9
- second_gate: bfloat16 [2048, 5632], P(None, ('kv', 'tp')), may hold values from -0.125 to 0.125
- second_up: bfloat16 [2048, 5632], P(None, ('kv', 'tp')), may hold values from -0.125 to 0.125
- second_down: bfloat16 [5632, 2048], P(('kv', 'tp')), may hold values from -0.078125 to 0.078125
Outputs:
- mixed_stream: bfloat16 [512, 2048], P('dp', ('kv', 'tp')), parts along dimension 0
- new_state: float32 [512, 8, 64, 128], P(('dp', 'kv'), 'tp'), parts along dimension 0
There are 4 independent parts, one for each index of `dp`. A program takes and returns all parts, laid end to end along the dimension named above; an argument that names none is the same for every part. Nothing has to cross between parts.
All inputs are finite; a program needn't handle non-finite values.
Results may differ from a plain program's by a relative error of at most 0.007.
Values may be sent and summed in bfloat16 or wider, within the bound.
A program may use at most 64 MiB of HBM per device.

v0:
```python
import math
import jax
import jax.numpy as jnp
from jax import lax
from jax.sharding import PartitionSpec as P

D = 2048
EPSILON = 1e-06
GATE_SOFTNESS = 16.0


def cut_along(value, dim, length):
    dims = value.shape
    parts = value.reshape(*dims[:dim], length, dims[dim] // length, *dims[dim + 1 :])
    return jnp.moveaxis(parts, dim, 0)


def summed_on_arrival(value, axis, dim):
    length = lax.axis_size(axis)
    parts = lax.all_to_all(cut_along(value, dim, length), axis, 0, 0, tiled=True)
    return jnp.sum(parts.astype(jnp.float32), axis=0)


def summed_on_arrival_2(value, axis, dim):
    parts = cut_along(value, dim, lax.axis_size(axis))
    arrived = lax.all_to_all(parts, axis, split_axis=0, concat_axis=0, tiled=True)
    return arrived.sum(axis=0)


def copy_for_each(value, axis):
    length = lax.axis_size(axis)
    return lax.all_to_all(
        jnp.broadcast_to(value[None], (length, *value.shape)), axis, 0, 0, tiled=True
    )


def in_order(parts, dim):
    dims = list(parts.shape[1:])
    dims[dim] *= parts.shape[0]
    return jnp.moveaxis(parts, 0, dim).reshape(dims)


def gathered_copies(value, axis, dim):
    parts = copy_for_each(value, axis)
    return in_order(parts, dim)


def in_one_piece(arrays, axis, dim, along):
    widths = [math.prod(a.shape[along:]) for a in arrays]
    both = jnp.concatenate(
        [a.reshape(*a.shape[:along], w) for a, w in zip(arrays, widths)], axis=along
    )
    result = summed_on_arrival_2(both, axis, dim)
    parts = jnp.split(result, [sum(widths[:k]) for k in range(1, len(widths))], axis=along)
    return tuple(
        (b.reshape(*result.shape[:along], *a.shape[along:]) for a, b in zip(arrays, parts))
    )


def half_block(stream, norm_gain, w_gate, w_up, w_down):
    wide = lax.all_gather(stream, ("kv", "tp"), axis=1, tiled=True).astype(jnp.float32)
    scaled = (wide * norm_gain).astype(jnp.bfloat16)
    gate_acc = jnp.dot(scaled, w_gate, preferred_element_type=jnp.float32)
    up_acc = jnp.dot(scaled, w_up, preferred_element_type=jnp.float32)
    square_acc = jnp.sum(wide * wide, axis=1)
    row_scale = lax.rsqrt(square_acc / norm_gain.shape[0] + EPSILON)[:, None]
    hidden = (jax.nn.silu(gate_acc * row_scale) * (up_acc * row_scale)).astype(jnp.bfloat16)
    partial_out = jnp.dot(hidden, w_down, preferred_element_type=jnp.float32)
    paired = summed_on_arrival(partial_out.astype(jnp.bfloat16), "tp", 0)
    blocked = summed_on_arrival_2(paired, "kv", 1)
    summed = lax.all_to_all(blocked, "tp", split_axis=1, concat_axis=0, tiled=True)
    return (stream.astype(jnp.float32) + 0.5 * summed).astype(jnp.bfloat16)


def body(
    stream,
    old_state,
    decay_amounts,
    first_gain,
    first_gate,
    first_up,
    first_down,
    mixer_gain,
    query_weight,
    key_weight,
    decay_weight,
    value_weight,
    output_gate_weight,
    head_gain,
    output_weight,
    second_gain,
    second_gate,
    second_up,
    second_down,
):
    middle = half_block(stream, first_gain, first_gate, first_up, first_down)
    paired_cols = gathered_copies(middle, "tp", 1)
    wide_cols = paired_cols.astype(jnp.float32)
    scaled = (wide_cols * mixer_gain).astype(jnp.bfloat16)
    query_part = jnp.dot(scaled, query_weight, preferred_element_type=jnp.float32)
    key_part = jnp.dot(scaled, key_weight, preferred_element_type=jnp.float32)
    decay_part = jnp.dot(scaled, decay_weight, preferred_element_type=jnp.float32)
    value_part = jnp.dot(scaled, value_weight, preferred_element_type=jnp.float32)
    outgate_part = jnp.dot(scaled, output_gate_weight, preferred_element_type=jnp.float32)
    local_rows = old_state.shape[0]
    local_heads = old_state.shape[1]
    key_dim = old_state.shape[2]
    value_dim = old_state.shape[3]
    query_sum, key_sum, decay_sum, value_sum, outgate_sum, own_squares = in_one_piece(
        (
            query_part,
            key_part,
            decay_part,
            value_part,
            outgate_part,
            jnp.sum(wide_cols * wide_cols, axis=1),
        ),
        "kv",
        0,
        1,
    )
    row_scale = lax.rsqrt(own_squares / D + EPSILON)[:, None]
    query = (query_sum * row_scale * key_dim ** (-0.5)).reshape(local_rows, local_heads, key_dim)
    keys = (key_sum * row_scale).reshape(local_rows, local_heads, key_dim)
    gate_logits = (decay_sum * row_scale).reshape(local_rows, local_heads, key_dim)
    values = (value_sum * row_scale).reshape(local_rows, local_heads, value_dim)
    decay_logarithm = jax.nn.log_sigmoid(gate_logits) / GATE_SOFTNESS - decay_amounts.reshape(
        local_rows, local_heads, key_dim
    )
    new_state = (
        jnp.exp(decay_logarithm)[..., None] * old_state + keys[..., None] * values[:, :, None, :]
    )
    readout = jnp.einsum("bhk,bhkv->bhv", query, new_state, precision=lax.Precision.HIGHEST)
    normed = readout * lax.rsqrt(jnp.mean(readout * readout, axis=-1, keepdims=True) + EPSILON)
    mixed_heads = (
        normed.reshape(local_rows, local_heads * value_dim)
        * head_gain
        * jax.nn.silu(outgate_sum * row_scale)
    ).astype(jnp.bfloat16)
    projected = jnp.dot(
        gathered_copies(mixed_heads, "kv", 0), output_weight, preferred_element_type=jnp.float32
    ).astype(jnp.bfloat16)
    attention_out = summed_on_arrival(
        lax.optimization_barrier(projected).astype(jnp.float32).astype(jnp.bfloat16), "tp", 1
    )
    after = (middle.astype(jnp.float32) + attention_out).astype(jnp.bfloat16)
    mixed_stream = half_block(after, second_gain, second_gate, second_up, second_down)
    return (mixed_stream, new_state)


def solution(mesh):
    in_specs = (
        P("dp", ("kv", "tp")),
        P(("dp", "kv"), "tp", None, None),
        P(("dp", "kv"), "tp"),
        P(),
        P(None, ("kv", "tp")),
        P(None, ("kv", "tp")),
        P(("kv", "tp"), None),
        P("kv"),
        P("kv", "tp"),
        P("kv", "tp"),
        P("kv", "tp"),
        P("kv", "tp"),
        P("kv", "tp"),
        P("tp"),
        P("tp", "kv"),
        P(),
        P(None, ("kv", "tp")),
        P(None, ("kv", "tp")),
        P(("kv", "tp"), None),
    )
    out_specs = (P("dp", ("kv", "tp")), P(("dp", "kv"), "tp", None, None))
    return jax.shard_map(body, mesh=mesh, in_specs=in_specs, out_specs=out_specs, check_vma=False)
```

profile of v0, /device:TPU:1, one launch (start us, length us, event | category | flops | bytes accessed | tf_op | source)
XLA Modules:
  0.0 385.9 jit_solution(13808392015291764144)
XLA Ops:
  0.6 91.5 %all_gather.6 = bf16[128,2048]{0,1:T(8,128)(2,1)S(1)} all-gather(bf16[128,16]{0,1:T(8,128)(2,1)} %param.19), channel_id=1, replica_groups=mesh['dp'=4,'kv'=64,'tp'=2] {'kv','tp'}, dimensions={1}, use_global_device_ids=true | all-gather | bytes 528384 | tf_op jit(solution)/shard_map/all_gather | solution.py:61
  92.2 0.3 fusion.5
  92.5 0.4 copy-done.13
  93.1 0.5 convolution_multiply_fusion.3
  93.6 0.4 copy-done.3
  94.0 0.8 convolution_convert_fusion.1
  94.8 3.9 %all_to_all.66 = bf16[2,64,2048]{2,1,0:T(8,128)(2,1)S(1)} all-to-all(bf16[2,64,2048]{2,1,0:T(8,128)(2,1)S(1)} %bitcast.78), channel_id=1, replica_groups=mesh['dp'=4,'kv'=64,'tp'=2] {'tp'}, dimensions={0} | all-to-all | bytes 1048576 | tf_op jit(solution)/shard_map/all_to_all | solution.py:20
  98.8 0.3 copy.89
  99.2 0.7 reshape.152
  99.9 40.3 %all_to_all.67 = f32[64,1,2048]{2,1,0:T(1,128)S(1)} all-to-all(f32[64,1,2048]{2,1,0:T(1,128)S(1)} %reshape.152), channel_id=1, replica_groups=mesh['dp'=4,'kv'=64,'tp'=2] {'kv'}, dimensions={0} | all-to-all | bytes 1048576 | tf_op jit(solution)/shard_map/all_to_all | solution.py:26
  140.1 0.5 broadcast.123
  140.6 1.9 reduce.4
  142.5 0.4 reshape.153
  143.1 6.1 %all_to_all.68 = f32[2,1,1024]{2,1,0:T(1,128)S(1)} all-to-all(f32[2,1,1024]{2,1,0:T(1,128)S(1)} %reshape.154), channel_id=1, replica_groups=mesh['dp'=4,'kv'=64,'tp'=2] {'tp'}, dimensions={0} | all-to-all | bytes 16384 | tf_op jit(solution)/shard_map/all_to_all | solution.py:71
  149.3 0.7 reduce.5
  150.1 0.6 copy-done.9
  150.7 3.7 all_to_all.69
  155.0 0.5 copy.93
  155.7 0.6 copy-done.10
  156.5 0.5 copy-done.11
  157.2 0.5 copy-done.12
  158.0 0.6 copy-done.6
  158.7 0.6 copy-done.7
  159.5 1.7 copy.94
  161.2 5.7 %all-to-all-start.4 = ((f32[64,2,1793]{2,1,0:T(2,128)}), f32[64,2,1793]{2,1,0:T(2,128)S(1)}, u32[]{:S(2)}, u32[]{:S(2)}) async-start(f32[64,2,1793]{2,1,0:T(2,128)} %copy.94), calls=%async_computation.4 | async-start | bytes 1966080 | tf_op jit(solution)/shard_map/all_to_all | solution.py:26
  167.0 49.8 %all-to-all-done.4 = f32[64,2,1793]{2,1,0:T(2,128)S(1)} async-done(((f32[64,2,1793]{2,1,0:T(2,128)}), f32[64,2,1793]{2,1,0:T(2,128)S(1)}, u32[]{:S(2)}, u32[]{:S(2)}) %all-to-all-start.4) | async-done | bytes 918048 | tf_op jit(solution)/shard_map/all_to_all | solution.py:26
  216.9 0.4 reduce_sum.94
  218.0 0.3 fusion.47
  218.5 0.6 copy-done.16
  219.3 23.2 %all_to_all.70 = bf16[64,2,512]{2,1,0:T(2,128)(2,1)S(1)} all-to-all(bf16[64,2,512]{2,1,0:T(2,128)(2,1)S(1)} %broadcast_in_dim.5), channel_id=1, replica_groups=mesh['dp'=4,'kv'=64,'tp'=2] {'kv'}, dimensions={0} | all-to-all | bytes 262144 | tf_op jit(solution)/shard_map/all_to_all | solution.py:32
  242.6 0.7 copy-done.8
  243.4 6.6 %all_to_all.71 = bf16[2,128,16]{1,2,0:T(8,128)(2,1)S(1)} all-to-all(bf16[2,128,16]{1,2,0:T(8,128)(2,1)S(1)} %bitcast.84), channel_id=1, replica_groups=mesh['dp'=4,'kv'=64,'tp'=2] {'tp'}, dimensions={0} | all-to-all | bytes 16384 | tf_op jit(solution)/shard_map/all_to_all | solution.py:20
  250.0 80.9 %all_gather.7 = bf16[128,2048]{0,1:T(8,128)(2,1)S(1)} all-gather(bf16[128,16]{0,1:T(8,128)(2,1)S(1)} %add_convert_fusion.1), channel_id=1, replica_groups=mesh['dp'=4,'kv'=64,'tp'=2] {'kv','tp'}, dimensions={1}, use_global_device_ids=true | all-gather | bytes 528384 | tf_op jit(solution)/shard_map/all_gather | solution.py:61
  330.9 0.3 fusion.7
  331.2 0.4 copy-done.14
  331.6 0.2 copy-done.19
  331.9 0.5 convolution_multiply_fusion.1
  332.4 0.5 copy-done.4
  332.9 0.8 convolution_convert_fusion
  333.7 3.9 %all_to_all.72 = bf16[2,64,2048]{2,1,0:T(8,128)(2,1)S(1)} all-to-all(bf16[2,64,2048]{2,1,0:T(8,128)(2,1)S(1)} %bitcast.79), channel_id=1, replica_groups=mesh['dp'=4,'kv'=64,'tp'=2] {'tp'}, dimensions={0} | all-to-all | bytes 1048576 | tf_op jit(solution)/shard_map/all_to_all | solution.py:20
  337.7 0.3 copy.96
  338.1 0.7 reshape.156
  338.7 37.1 %all_to_all.73 = f32[64,1,2048]{2,1,0:T(1,128)S(1)} all-to-all(f32[64,1,2048]{2,1,0:T(1,128)S(1)} %reshape.156), channel_id=1, replica_groups=mesh['dp'=4,'kv'=64,'tp'=2] {'kv'}, dimensions={0} | all-to-all | bytes 1048576 | tf_op jit(solution)/shard_map/all_to_all | solution.py:26
  375.8 1.9 reduce.6
  377.7 0.4 reshape.157
  378.3 6.1 %all_to_all.74 = f32[2,1,1024]{2,1,0:T(1,128)S(1)} all-to-all(f32[2,1,1024]{2,1,0:T(1,128)S(1)} %reshape.158), channel_id=1, replica_groups=mesh['dp'=4,'kv'=64,'tp'=2] {'tp'}, dimensions={0} | all-to-all | bytes 16384 | tf_op jit(solution)/shard_map/all_to_all | solution.py:71
  384.4 0.7 reduce.7
  385.3 0.6 add_convert_fusion
  (77 shorter events, 4.3 us)
Async XLA Ops:
  0.6 92.9 %copy-start = (bf16[44,2048]{1,0:T(8,128)(2,1)S(1)}, bf16[44,2048]{1,0:T(8,128)(2,1)}, u32[]{:S(2)}) copy-start(bf16[44,2048]{1,0:T(8,128)(2,1)} %param.25) | copy-start | bytes 540676
  92.2 0.7 copy-start.13
  92.2 0.9 copy-start.18
  93.1 0.9 copy-start.3
  150.0 0.7 copy-start.9
  155.0 0.7 copy-start.17
  155.6 0.7 copy-start.10
  156.3 0.7 copy-start.11
  157.1 0.7 copy-start.12
  157.8 0.8 copy-start.6
  158.5 0.8 copy-start.7
  161.2 5.7 %copy-start.15 = (f32[2,256]{1,0:T(2,128)S(1)}, f32[2,256]{1,0:T(2,128)}, u32[]{:S(2)}) copy-start(f32[2,256]{1,0:T(2,128)} %param.21) | copy-start | bytes 6148
  161.2 55.6 %all-to-all-start.4 = ((f32[64,2,1793]{2,1,0:T(2,128)}), f32[64,2,1793]{2,1,0:T(2,128)S(1)}, u32[]{:S(2)}, u32[]{:S(2)}) async-start(f32[64,2,1793]{2,1,0:T(2,128)} %copy.94), calls=%async_computation.4 | async-start | bytes 1966080 | tf_op jit(solution)/shard_map/all_to_all | solution.py:26
  167.0 50.8 %copy-start.2 = (f32[2,4,64,128]{3,2,1,0:T(8,128)S(1)}, f32[2,4,64,128]{3,2,1,0:T(8,128)}, u32[]{:S(2)}) copy-start(f32[2,4,64,128]{3,2,1,0:T(8,128)} %param.20) | copy-start | bytes 786436
  218.0 24.5 %copy-start.1 = (f32[2,4,64,128]{3,2,1,0:T(8,128)}, f32[2,4,64,128]{3,2,1,0:T(8,128)S(1)}, u32[]{:S(2)}) copy-start(f32[2,4,64,128]{3,2,1,0:T(8,128)S(1)} %multiply_add_fusion) | copy-start | bytes 786436
  218.4 0.7 copy-start.16
  242.5 0.8 copy-start.8
  330.9 0.7 copy-start.14
  330.9 0.9 copy-start.19
  331.9 0.9 copy-start.4
  331.9 1.0 copy-start.5
where the time goes:
time: 387 us; the launch traced here: 386 us
  blocking collectives  303 us (78%)
  waiting for transfers between devices  49.8 us (13%)
  local copies, waits for them, and re-layouts  14.2 us (4%)
  other arithmetic  7.92 us (2%)
  starting transfers between devices  5.69 us (1%)
    all_gather x2, blocking collectives, half_block(): lax.all_gather(stream, ('kv', 'tp'), axis=1, tiled=True).astype(jnp.float32)  172 us
    all_to_all x2, blocking collectives, summed_on_arrival_2(): lax.all_to_all(parts, axis, split_axis=0, concat_axis=0, tiled=True)  77.4 us
    all_to_all x1, waiting for transfers between devices, summed_on_arrival_2(): lax.all_to_all(parts, axis, split_axis=0, concat_axis=0, tiled=True)  49.8 us
    all_to_all x2, blocking collectives, copy_for_each(): lax.all_to_all(jnp.broadcast_to(value[None], (length, *value.shape)), axi...  26.9 us
    all_to_all x3, blocking collectives, summed_on_arrival(): lax.all_to_all(cut_along(value, dim, length), axis, 0, 0, tiled=True)  14.5 us
    all_to_all x2, blocking collectives, half_block(): lax.all_to_all(blocked, 'tp', split_axis=1, concat_axis=0, tiled=True)  12.3 us
    unnamed x48, local copies, waits for them, and re-layouts  9.68 us
  transfers between devices with their start and end apart: 1, of which 1 were waited for; matrix products, arithmetic and copies ran while one was open for 0% of the time, Pallas kernels for 0%

commit v1 on v0

--- a/solution.py
+++ b/solution.py
@@ -7,6 +7,13 @@
 D = 2048
 EPSILON = 1e-06
 GATE_SOFTNESS = 16.0
+
+
+def all_by_exchange(x, mesh_axis, dim):
+    peers = lax.axis_size(mesh_axis)
+    shards = jnp.stack([x for _ in range(peers)])
+    shards = lax.all_to_all(shards, mesh_axis, split_axis=0, concat_axis=0)
+    return jnp.concatenate(shards, axis=dim)
 
 
 def cut_along(value, dim, length):
@@ -58,7 +65,7 @@
 
 
 def half_block(stream, norm_gain, w_gate, w_up, w_down):
-    wide = lax.all_gather(stream, ("kv", "tp"), axis=1, tiled=True).astype(jnp.float32)
+    wide = all_by_exchange(stream, ("kv", "tp"), 1).astype(jnp.float32)
     scaled = (wide * norm_gain).astype(jnp.bfloat16)
     gate_acc = jnp.dot(scaled, w_gate, preferred_element_type=jnp.float32)
     up_acc = jnp.dot(scaled, w_up, preferred_element_type=jnp.float32)

time: 387 us -> 304 us (0.79)
  blocking collectives: 303 us -> 219 us
    all_gather x2 -> x0, blocking collectives: 172 us -> none  [half_block(): lax.all_gather(stream, ('kv', 'tp'), axis=1, tiled=True).astype(jnp.float32)]
    all_to_all x0 -> x2, blocking collectives: none -> 87.3 us  [all_by_exchange(): shards = lax.all_to_all(shards, mesh_axis, split_axis=0, concat_axis=0)]
where the time goes in v1:
time: 304 us; the launch traced here: 303 us
  blocking collectives  219 us (72%)
  waiting for transfers between devices  49.8 us (16%)
  local copies, waits for them, and re-layouts  16.3 us (5%)
  other arithmetic  8.59 us (3%)
  starting transfers between devices  5.69 us (2%)
    all_to_all x2, blocking collectives, all_by_exchange(): shards = lax.all_to_all(shards, mesh_axis, split_axis=0, concat_axis=0)  87.3 us
    all_to_all x2, blocking collectives, summed_on_arrival_2(): lax.all_to_all(parts, axis, split_axis=0, concat_axis=0, tiled=True)  76.8 us
    all_to_all x1, waiting for transfers between devices, summed_on_arrival_2(): lax.all_to_all(parts, axis, split_axis=0, concat_axis=0, tiled=True)  49.8 us
    all_to_all x2, blocking collectives, copy_for_each(): lax.all_to_all(jnp.broadcast_to(value[None], (length, *value.shape)), axi...  26.7 us
    all_to_all x3, blocking collectives, summed_on_arrival(): lax.all_to_all(cut_along(value, dim, length), axis, 0, 0, tiled=True)  15.9 us
    all_to_all x2, blocking collectives, half_block(): lax.all_to_all(blocked, 'tp', split_axis=1, concat_axis=0, tiled=True)  12.3 us
    unnamed x48, local copies, waits for them, and re-layouts  10.9 us
  transfers between devices with their start and end apart: 1, of which 1 were waited for; matrix products, arithmetic and copies ran while one was open for 0% of the time, Pallas kernels for 0%

profile of v1, /device:TPU:1, one launch (start us, length us, event | category | flops | bytes accessed | tf_op | source)
XLA Modules:
  0.0 303.2 jit_solution(17707296578034100339)
XLA Ops:
  0.6 0.8 stack.4
  1.4 51.0 %all_to_all.76 = bf16[128,128,16]{1,2,0:T(8,128)(2,1)S(1)} all-to-all(bf16[128,128,16]{1,2,0:T(8,128)(2,1)S(1)} %stack.4), channel_id=1, replica_groups=mesh['dp'=4,'kv'=64,'tp'=2] {'kv','tp'}, dimensions={0} | all-to-all | bytes 1048576 | tf_op jit(solution)/shard_map/all_to_all | solution.py:15
  52.8 0.4 copy-done.15
  53.2 0.3 fusion.5
  53.5 0.6 copy-done.3
  54.3 0.7 copy-done.5
  55.0 0.5 convolution_convert_fusion.1
  55.6 4.9 %all_to_all.77 = bf16[2,64,2048]{2,1,0:T(8,128)(2,1)S(1)} all-to-all(bf16[2,64,2048]{2,1,0:T(8,128)(2,1)S(1)} %bitcast.94), channel_id=1, replica_groups=mesh['dp'=4,'kv'=64,'tp'=2] {'tp'}, dimensions={0} | all-to-all | bytes 1048576 | tf_op jit(solution)/shard_map/all_to_all | solution.py:27
  60.5 0.3 copy.91
  60.9 0.7 reshape.166
  61.5 38.3 %all_to_all.78 = f32[64,1,2048]{2,1,0:T(1,128)S(1)} all-to-all(f32[64,1,2048]{2,1,0:T(1,128)S(1)} %reshape.166), channel_id=1, replica_groups=mesh['dp'=4,'kv'=64,'tp'=2] {'kv'}, dimensions={0} | all-to-all | bytes 1048576 | tf_op jit(solution)/shard_map/all_to_all | solution.py:33
  99.9 0.5 broadcast.127
  100.4 1.9 reduce.8
  102.3 0.4 reshape.167
  102.9 6.1 %all_to_all.79 = f32[2,1,1024]{2,1,0:T(1,128)S(1)} all-to-all(f32[2,1,1024]{2,1,0:T(1,128)S(1)} %reshape.168), channel_id=1, replica_groups=mesh['dp'=4,'kv'=64,'tp'=2] {'tp'}, dimensions={0} | all-to-all | bytes 16384 | tf_op jit(solution)/shard_map/all_to_all | solution.py:78
  109.0 0.7 reduce.9
  109.9 0.6 copy-done.11
  110.5 3.7 %all_to_all.80 = bf16[2,128,16]{1,2,0:T(8,128)(2,1)S(1)} all-to-all(bf16[2,128,16]{1,2,0:T(8,128)(2,1)S(1)} %broadcast_in_dim.4), channel_id=1, replica_groups=mesh['dp'=4,'kv'=64,'tp'=2] {'tp'}, dimensions={0} | all-to-all | bytes 16384 | tf_op jit(solution)/shard_map/all_to_all | solution.py:39
  114.7 0.5 copy.95
  115.4 0.6 copy-done.12
  116.3 0.5 copy-done.13
  117.0 0.5 copy-done.14
  117.7 0.6 copy-done.8
  118.5 0.5 copy-done.9
  119.3 1.7 copy.96
  121.0 5.7 %all-to-all-start.5 = ((f32[64,2,1793]{2,1,0:T(2,128)}), f32[64,2,1793]{2,1,0:T(2,128)S(1)}, u32[]{:S(2)}, u32[]{:S(2)}) async-start(f32[64,2,1793]{2,1,0:T(2,128)} %copy.96), calls=%async_computation.5 | async-start | bytes 1966080 | tf_op jit(solution)/shard_map/all_to_all | solution.py:33
  126.8 49.8 %all-to-all-done.5 = f32[64,2,1793]{2,1,0:T(2,128)S(1)} async-done(((f32[64,2,1793]{2,1,0:T(2,128)}), f32[64,2,1793]{2,1,0:T(2,128)S(1)}, u32[]{:S(2)}, u32[]{:S(2)}) %all-to-all-start.5) | async-done | bytes 918048 | tf_op jit(solution)/shard_map/all_to_all | solution.py:33
  176.6 0.4 reduce_sum.94
  177.8 0.3 fusion.39
  178.3 0.6 copy-done.18
  179.0 23.0 %all_to_all.81 = bf16[64,2,512]{2,1,0:T(2,128)(2,1)S(1)} all-to-all(bf16[64,2,512]{2,1,0:T(2,128)(2,1)S(1)} %broadcast_in_dim.5), channel_id=1, replica_groups=mesh['dp'=4,'kv'=64,'tp'=2] {'kv'}, dimensions={0} | all-to-all | bytes 262144 | tf_op jit(solution)/shard_map/all_to_all | solution.py:39
  202.2 0.7 copy-done.10
  203.0 6.6 %all_to_all.82 = bf16[2,128,16]{1,2,0:T(8,128)(2,1)S(1)} all-to-all(bf16[2,128,16]{1,2,0:T(8,128)(2,1)S(1)} %bitcast.100), channel_id=1, replica_groups=mesh['dp'=4,'kv'=64,'tp'=2] {'tp'}, dimensions={0} | all-to-all | bytes 16384 | tf_op jit(solution)/shard_map/all_to_all | solution.py:27
  209.6 36.2 %all_to_all.83 = bf16[128,128,16]{1,2,0:T(8,128)(2,1)S(1)} all-to-all(bf16[128,128,16]{1,2,0:T(8,128)(2,1)S(1)} %stack.5), channel_id=1, replica_groups=mesh['dp'=4,'kv'=64,'tp'=2] {'kv','tp'}, dimensions={0} | all-to-all | bytes 1048576 | tf_op jit(solution)/shard_map/all_to_all | solution.py:15
  246.2 0.4 copy-done.16
  246.6 0.3 fusion.4
  246.9 0.6 copy-done.4
  247.7 0.7 copy-done.6
  248.5 0.5 convolution_convert_fusion
  249.1 4.5 %all_to_all.84 = bf16[2,64,2048]{2,1,0:T(8,128)(2,1)S(1)} all-to-all(bf16[2,64,2048]{2,1,0:T(8,128)(2,1)S(1)} %bitcast.95), channel_id=1, replica_groups=mesh['dp'=4,'kv'=64,'tp'=2] {'tp'}, dimensions={0} | all-to-all | bytes 1048576 | tf_op jit(solution)/shard_map/all_to_all | solution.py:27
  253.6 0.3 copy.98
  254.0 0.7 reshape.170
  254.6 38.4 %all_to_all.85 = f32[64,1,2048]{2,1,0:T(1,128)S(1)} all-to-all(f32[64,1,2048]{2,1,0:T(1,128)S(1)} %reshape.170), channel_id=1, replica_groups=mesh['dp'=4,'kv'=64,'tp'=2] {'kv'}, dimensions={0} | all-to-all | bytes 1048576 | tf_op jit(solution)/shard_map/all_to_all | solution.py:33
  293.1 1.9 reduce.10
  295.0 0.4 reshape.171
  295.6 6.1 %all_to_all.86 = f32[2,1,1024]{2,1,0:T(1,128)S(1)} all-to-all(f32[2,1,1024]{2,1,0:T(1,128)S(1)} %reshape.172), channel_id=1, replica_groups=mesh['dp'=4,'kv'=64,'tp'=2] {'tp'}, dimensions={0} | all-to-all | bytes 16384 | tf_op jit(solution)/shard_map/all_to_all | solution.py:78
  301.7 0.7 reduce.11
  302.6 0.6 add_convert_fusion
  (81 shorter events, 5.1 us)
Async XLA Ops:
  0.6 53.7 %copy-start = (bf16[44,2048]{1,0:T(8,128)(2,1)S(1)}, bf16[44,2048]{1,0:T(8,128)(2,1)}, u32[]{:S(2)}) copy-start(bf16[44,2048]{1,0:T(8,128)(2,1)} %param.25) | copy-start | bytes 540676
  52.5 0.7 copy-start.15
  53.2 0.9 copy-start.3
  54.1 0.9 copy-start.5
  109.8 0.7 copy-start.11
  114.7 0.7 copy-start.19
  115.4 0.7 copy-start.12
  116.1 0.7 copy-start.13
  116.8 0.7 copy-start.14
  117.5 0.8 copy-start.8
  118.3 0.8 copy-start.9
  121.0 5.7 %copy-start.17 = (f32[2,256]{1,0:T(2,128)S(1)}, f32[2,256]{1,0:T(2,128)}, u32[]{:S(2)}) copy-start(f32[2,256]{1,0:T(2,128)} %param.21) | copy-start | bytes 6148
  121.0 55.6 %all-to-all-start.5 = ((f32[64,2,1793]{2,1,0:T(2,128)}), f32[64,2,1793]{2,1,0:T(2,128)S(1)}, u32[]{:S(2)}, u32[]{:S(2)}) async-start(f32[64,2,1793]{2,1,0:T(2,128)} %copy.96), calls=%async_computation.5 | async-start | bytes 1966080 | tf_op jit(solution)/shard_map/all_to_all | solution.py:33
  126.8 50.8 %copy-start.2 = (f32[2,4,64,128]{3,2,1,0:T(8,128)S(1)}, f32[2,4,64,128]{3,2,1,0:T(8,128)}, u32[]{:S(2)}) copy-start(f32[2,4,64,128]{3,2,1,0:T(8,128)} %param.20) | copy-start | bytes 786436
  177.8 24.3 %copy-start.1 = (f32[2,4,64,128]{3,2,1,0:T(8,128)}, f32[2,4,64,128]{3,2,1,0:T(8,128)S(1)}, u32[]{:S(2)}) copy-start(f32[2,4,64,128]{3,2,1,0:T(8,128)S(1)} %multiply_add_fusion) | copy-start | bytes 786436
  178.2 0.7 copy-start.18
  202.1 0.8 copy-start.10
  245.9 0.7 copy-start.16
  246.6 0.9 copy-start.4
  247.5 0.9 copy-start.6
  247.5 1.0 copy-start.7
